TPU v7x, 32 devices: a whole 2x2x4 slice. The times are simulated.
32 devices in a mesh: sp: 8 (over z, x), tp: 4 (over y, core).
Axes of the slice: x: 2, y: 2, z: 4, core: 2. Of those that a mesh axis runs over, the one named last changes fastest.
Arguments:
- queries: bfloat16 [4096, 512], P('sp', 'tp'), may hold values from -9.5625 to 9.5625
- keys: bfloat16 [4096, 512], P('sp', 'tp'), may hold values from -9.5625 to 9.5625
- values: bfloat16 [4096, 512], P('sp', 'tp'), may hold values from -6 to 6
- key_bias: bfloat16 [4096, 8], P('sp', 'tp'), may hold values from -17 to 0
- residual: bfloat16 [4096, 2048], P(('sp', 'tp')), may hold values from -6 to 6
- out_weight: bfloat16 [512, 2048], replicated, may hold values from -1 to 1
- norm_gain: float32 [2048], replicated, may hold values from 0.1 to 1.9
- routes: int32 [4096, 2], P(('sp', 'tp')), may hold values from 0 to 7, all different within a row; in each aligned block of 128 rows (0 to 127, 128 to 255, ...) at most 40 rows name the same one
- route_weights: float32 [4096, 2], P(('sp', 'tp')), may hold values from 0.25 to 2
- gate_weight: bfloat16 [8, 2048, 4096], P('sp', None, 'tp'), may hold values from -0.125 to 0.125
- up_weight: bfloat16 [8, 2048, 4096], P('sp', None, 'tp'), may hold values from -0.125 to 0.125
- down_weight: bfloat16 [8, 4096, 2048], P('sp', 'tp'), may hold values from -0.09375 to 0.09375
Outputs:
- output: bfloat16 [4096, 2048], P(('sp', 'tp'))
Inputs may be any that keep to these rules, and one draw needn't show every extreme that they name: `routes`: each row names 2 different experts; the rows of one device name no expert more than 40 times.
All inputs are finite; a program needn't handle non-finite values.
Results may differ from a plain program's by a relative error of at most 0.017.
Values may be sent and summed in bfloat16 or wider, within the bound.
A program may use at most 128 MiB of HBM per device.

v0:
```python
import jax
import jax.numpy as jnp
from jax import lax
from jax.sharding import PartitionSpec as P

HEAD_DIM = 64
TOP = 2
SPAN = 512
epsilon = 1e-06


def shards(
    queries,
    keys,
    values,
    key_bias,
    residual,
    out_weight,
    norm_gain,
    routes,
    route_weights,
    gate_weight,
    up_weight,
    down_weight,
):
    shard_len = queries.shape[0]
    local_heads = key_bias.shape[1]
    sp_count = lax.axis_size("sp")
    offset = lax.axis_index("sp") * shard_len
    query_heads = queries.reshape(shard_len, local_heads, HEAD_DIM)
    query_pos = offset + lax.iota(jnp.int32, shard_len)
    score_scale = HEAD_DIM ** (-0.5)
    slot_count = sp_count * shard_len // SPAN

    def span_terms(key_rows, value_rows, bias_rows, key_first):
        scores = jnp.einsum(
            "qhd,khd->qhk",
            query_heads,
            key_rows.reshape(SPAN, local_heads, HEAD_DIM),
            preferred_element_type=jnp.float32,
        )
        scores = scores * score_scale + jnp.transpose(bias_rows.astype(jnp.float32))[None, :, :]
        key_pos = key_first + lax.iota(jnp.int32, SPAN)
        earlier = key_pos[None, None, :] < query_pos[:, None, None]
        failure = jnp.where(earlier, jax.nn.log_sigmoid(-scores), 0.0)
        later_sum = lax.cumsum(failure, axis=2, reverse=True) - failure
        weights = jnp.where(earlier, jnp.exp(jax.nn.log_sigmoid(scores) + later_sum), 0.0).astype(
            jnp.bfloat16
        )
        span_out = jnp.einsum(
            "qhk,khd->qhd",
            weights,
            value_rows.reshape(SPAN, local_heads, HEAD_DIM),
            preferred_element_type=jnp.float32,
        )
        return (span_out, jnp.sum(failure, axis=2))

    def skipped():
        return (
            jnp.zeros((shard_len, local_heads, HEAD_DIM), jnp.float32),
            jnp.zeros((shard_len, local_heads), jnp.float32),
        )

    empty_pair = (
        jnp.zeros((slot_count, shard_len, local_heads, HEAD_DIM), jnp.float32),
        jnp.zeros((slot_count, shard_len, local_heads), jnp.float32),
    )
    key_piece = lax.all_gather(keys, "sp", axis=0, tiled=True)
    value_piece = lax.all_gather(values, "sp", axis=0, tiled=True)
    bias_piece = lax.all_gather(key_bias, "sp", axis=0, tiled=True)
    span_total = key_piece.shape[0] // SPAN

    def place_span(which, held):
        outs_held, totals_held = held
        row_begin = which * SPAN

        def compute():
            return span_terms(
                lax.dynamic_slice_in_dim(key_piece, row_begin, SPAN, 0),
                lax.dynamic_slice_in_dim(value_piece, row_begin, SPAN, 0),
                lax.dynamic_slice_in_dim(bias_piece, row_begin, SPAN, 0),
                row_begin,
            )

        span_out, span_sum = lax.cond(row_begin < offset + shard_len, compute, skipped)
        slot = row_begin // SPAN
        return (
            lax.dynamic_update_index_in_dim(outs_held, span_out, slot, 0),
            lax.dynamic_update_index_in_dim(totals_held, span_sum, slot, 0),
        )

    span_outs, span_sums = lax.fori_loop(0, span_total, place_span, empty_pair)
    after_span = lax.cumsum(span_sums, axis=0, reverse=True) - span_sums
    attended = jnp.sum(jnp.exp(after_span)[..., None] * span_outs, axis=0)
    attended = attended.reshape(shard_len, local_heads * HEAD_DIM).astype(jnp.bfloat16)
    token_heads = lax.all_to_all(attended, "tp", split_axis=0, concat_axis=1, tiled=True)
    projected = jnp.dot(token_heads, out_weight, preferred_element_type=jnp.float32)
    stream = (residual.astype(jnp.float32) + projected).astype(jnp.bfloat16).astype(jnp.float32)
    normed = (
        stream * lax.rsqrt(jnp.mean(stream * stream, axis=-1, keepdims=True) + epsilon) * norm_gain
    ).astype(jnp.bfloat16)
    token_count = residual.shape[0]
    width_model = residual.shape[1]
    capacity = max(2, 5 * token_count * TOP // (4 * sp_count))
    flat_routes = routes.reshape(-1)
    onehot = (flat_routes[:, None] == lax.iota(jnp.int32, sp_count)[None, :]).astype(jnp.int32)
    before = jnp.cumsum(onehot, axis=0) - onehot
    slot_of = flat_routes * capacity + jnp.sum(before * onehot, axis=1)
    select = (slot_of[:, None] == lax.iota(jnp.int32, sp_count * capacity)[None, :]).astype(
        jnp.bfloat16
    )
    placing = jnp.sum(select.reshape(token_count, TOP, sp_count * capacity), axis=1)
    outgoing = jnp.einsum("ts,td->sd", placing, normed, preferred_element_type=jnp.float32).astype(
        jnp.bfloat16
    )
    arrived = lax.all_to_all(outgoing, "sp", split_axis=0, concat_axis=0, tiled=True)
    row_block = lax.all_gather(arrived, "tp", axis=0, tiled=True)
    gate_act = jnp.dot(row_block, gate_weight[0], preferred_element_type=jnp.float32)
    up_act = jnp.dot(row_block, up_weight[0], preferred_element_type=jnp.float32)
    hidden = (jax.nn.silu(gate_act) * up_act).astype(jnp.bfloat16)
    partial_value = jnp.dot(hidden, down_weight[0], preferred_element_type=jnp.float32)
    summed = lax.psum_scatter(
        lax.optimization_barrier(partial_value.astype(jnp.bfloat16))
        .astype(jnp.float32)
        .astype(jnp.bfloat16),
        "tp",
        scatter_dimension=0,
        tiled=True,
    )
    returned = lax.all_to_all(summed, "sp", split_axis=0, concat_axis=0, tiled=True)
    picked = jnp.dot(select, returned, preferred_element_type=jnp.float32).reshape(
        token_count, TOP, width_model
    )
    routed = jnp.sum(picked * route_weights[:, :, None], axis=1)
    return (stream + routed).astype(jnp.bfloat16)


def solution(mesh):
    return jax.shard_map(
        shards,
        mesh=mesh,
        in_specs=(
            P("sp", "tp"),
            P("sp", "tp"),
            P("sp", "tp"),
            P("sp", "tp"),
            P(("sp", "tp"), None),
            P(),
            P(),
            P(("sp", "tp"), None),
            P(("sp", "tp"), None),
            P("sp", None, "tp"),
            P("sp", None, "tp"),
            P("sp", "tp", None),
        ),
        out_specs=P(("sp", "tp"), None),
        check_vma=False,
    )
```

profile of v0, /device:TPU:0, one launch (start us, length us, event | category | flops | bytes accessed | tf_op | source)
XLA Modules:
  0.0 488.3 jit_solution(3065898955620560094)
XLA Ops:
  6.5 1.8 copy.63
  8.4 1.7 copy.62
  10.1 0.8 copy.66
  12.3 1.0 copy.64
  13.4 28.3 %all_gather.14 = bf16[4096,2]{0,1:T(2,128)(2,1)S(1)} all-gather(bf16[512,2]{0,1:T(2,128)(2,1)} %param.19), channel_id=1, replica_groups=mesh['sp'=8,'tp'=4] {'sp'}, dimensions={0}, use_global_device_ids=true | all-gather | bytes 18432 | tf_op jit(solution)/shard_map/all_gather | solution.py:70
  42.3 9.2 %all-gather.6.cloned.1.call-done = bf16[4096,128]{0,1:T(8,128)(2,1)} async-done(((bf16[512,128]{0,1:T(8,128)(2,1)}), bf16[4096,128]{0,1:T(8,128)(2,1)}) %all-gather.6.cloned.1.call-update) | async-done | bytes 1048592 | tf_op jit(solution)/shard_map/all_gather | solution.py:68
  51.6 40.3 %all-gather.4.cloned.1.call-done = bf16[4096,128]{0,1:T(8,128)(2,1)} async-done(((bf16[512,128]{0,1:T(8,128)(2,1)}), bf16[4096,128]{0,1:T(8,128)(2,1)}) %all-gather.4.cloned.1.call-update) | async-done | bytes 1048592 | tf_op jit(solution)/shard_map/all_gather | solution.py:69
  91.9 1.6 broadcast_in_dim.56
  93.5 28.5 %while.18 = (s32[]{:T(128)}, f32[8,512,2,64]{1,3,2,0:T(8,128)}, f32[8,512,2]{1,2,0:T(2,128)S(1)}, s32[]{:T(128)}, bf16[4096,128]{0,1:T(8,128)(2,1)}, /*index=5*/...) while((s32[]{:T(128)}, f32[8,512,2,64]{1,3,2,0:T(8,128)}, ...), condition=%wide.region_6.7_spmd.clone, body=%wide.region_0.6_spmd.clone.sunk | while | flops 218906624 | bytes 42494496 | solution.py:92
  93.5 22.3 %conditional.3 = (f32[1,512,2,64]{1,3,2,0:T(8,128)S(1)}, f32[1,512,2]{1,2,0:T(2,128)S(1)}) conditional(s32[]{:T(128)} %convert_element_type.94, () %tuple.60, (s32[]{:T(128)}, bf16[4096,128]{0,1:T(8,128)(2,1)}, s32[]{:T(128)}, bf16[4096,128]{0,1:T(8,128)(2,1)}, bf16[512,2,64]{0,2,1:T(8,128)(2,1)S(1)}, /*index=5*/bf16[4096,2]{0,1:T(2,128)(2,1)S(1)}, ...), branch_computations={%region_1.0_spmd, %region_2.5_spmd} | conditional | flops 218906624 | bytes 41959552 | solution.py:85
  93.5 1.0 constant_dynamic-slice_fusion
  94.7 3.0 fusion.15
  97.8 9.6 %fusion.13 = f32[512,2,4,128]{0,2,1,3:T(4,128)S(1)} fusion(f32[512,2,4,128]{0,3,2,1:T(8,128)S(1)} %bitcast.89), kind=kOutput, calls=%fused_computation.18 | output fusion | flops 66584576 | bytes 4194304 | tf_op jit(solution)/shard_map/reduce-window
  107.4 1.3 copy-done.1
  108.8 1.8 broadcast_add_fusion
  110.6 1.2 copy.60
  112.2 3.2 fusion.6
  118.1 0.7 constant_dynamic-update-slice_fusion.4
  118.9 0.7 constant_dynamic-update-slice_fusion.4
  119.7 0.7 constant_dynamic-update-slice_fusion.4
  122.0 1.8 multiply_reduce_fusion
  124.6 3.5 all-to-all-start
  128.2 4.5 all-to-all-done
  132.6 1.6 multiply_reduce_fusion.1
  134.8 190.0 %all_to_all.40 = bf16[8,40,2048]{2,1,0:T(8,128)(2,1)} all-to-all(bf16[8,40,2048]{2,1,0:T(8,128)(2,1)S(1)} %bitcast.92), channel_id=1, replica_groups=mesh['sp'=8,'tp'=4] {'sp'}, dimensions={0} | all-to-all | bytes 2621440 | tf_op jit(solution)/shard_map/all_to_all | solution.py:116
  324.9 38.8 %all-gather.8.cloned.1.call-done = bf16[1280,2048]{1,0:T(8,128)(2,1)} async-done(((bf16[320,2048]{1,0:T(8,128)(2,1)}), bf16[1280,2048]{1,0:T(8,128)(2,1)}) %all-gather.8.cloned.1.call-update) | async-done | bytes 5242896 | tf_op jit(solution)/shard_map/all_gather | solution.py:117
  363.7 10.2 %fusion.18 = f32[1280,1024]{1,0:T(8,128)} fusion(bf16[1280,2048]{1,0:T(8,128)(2,1)} %all-gather.8.cloned.1.call-done, bf16[1,2048,1024]{2,1,0:T(8,128)(2,1)} %param.25), kind=kOutput, calls=%fused_computation.37 | convolution fusion | flops 5368709120 | bytes 14680064 | tf_op jit(solution)/shard_map/dot_general | solution.py:118
  373.9 18.0 %convolution_convert_fusion = bf16[1280,2048]{1,0:T(8,128)(2,1)} fusion(bf16[1,1024,2048]{2,1,0:T(8,128)(2,1)} %param.27, f32[1280,1024]{1,0:T(8,128)} %fusion.18, bf16[1280,2048]{1,0:T(8,128)(2,1)} %all-gather.8.cloned.1.call-done, bf16[1,2048,1024]{2,1,0:T(8,128)(2,1)} %param.26), kind=kOutput, calls=%fused_computation.33 | convolution fusion | flops 10747904000 | bytes 24117248 | tf_op jit(solution)/shard_map/dot_general | solution.py:121
  391.9 51.5 %reduce-scatter.2.cloned.1.call-done = bf16[320,2048]{1,0:T(8,128)(2,1)} async-done(((bf16[1280,2048]{1,0:T(8,128)(2,1)}), bf16[320,2048]{1,0:T(8,128)(2,1)}) %reduce-scatter.2.cloned.1.call-update) | async-done | bytes 1310736 | tf_op jit(solution)/shard_map/reduce_scatter | solution.py:122
  443.4 36.7 %all_to_all.41 = bf16[8,40,2048]{2,1,0:T(8,128)(2,1)S(1)} all-to-all(bf16[8,40,2048]{2,1,0:T(8,128)(2,1)} %bitcast.95), channel_id=1, replica_groups=mesh['sp'=8,'tp'=4] {'sp'}, dimensions={0} | all-to-all | bytes 2621440 | tf_op jit(solution)/shard_map/all_to_all | solution.py:130
  480.1 0.8 fusion.24
  480.9 0.9 add_convert_fusion
  (84 shorter events, 8.7 us)
Async XLA Ops:
  6.5 126.1 %copy-start = (bf16[512,2048]{1,0:T(8,128)(2,1)S(1)}, bf16[512,2048]{1,0:T(8,128)(2,1)}, u32[]{:S(2)}) copy-start(bf16[512,2048]{1,0:T(8,128)(2,1)} %param.21) | copy-start | bytes 6291460
  6.5 45.0 %all-gather.6.cloned.1.call-start = ((), (), s32[]{:S(2)}) async-start(), calls=%async_computation.5 | async-start | bytes 1179648 | tf_op jit(solution)/shard_map/all_gather | solution.py:68
  8.4 83.5 %all-gather.4.cloned.1.call-start = ((), (), s32[]{:S(2)}) async-start(), calls=%async_computation.4 | async-start | bytes 1179648 | tf_op jit(solution)/shard_map/all_gather | solution.py:69
  107.4 1.3 copy-start.1
  110.6 1.6 copy-start.2
  124.6 9.6 %copy-start.3 = (f32[2048]{0:T(1024)S(1)}, f32[2048]{0:T(1024)}, u32[]{:S(2)}) copy-start(f32[2048]{0:T(1024)} %param.22) | copy-start | bytes 24580
  124.6 8.0 %all-to-all-start = ((bf16[4,128,128]{1,2,0:T(8,128)(2,1)}), bf16[4,128,128]{1,2,0:T(8,128)(2,1)S(1)}, u32[]{:S(2)}, u32[]{:S(2)}) async-start(bf16[4,128,128]{1,2,0:T(8,128)(2,1)} %copy.65), calls=%async_computation | async-start | bytes 262144 | tf_op jit(solution)/shard_map/all_to_all | solution.py:96
  128.1 235.7 %all-gather.8.cloned.1.call-start = ((), (), s32[]{:S(2)}) async-start(), calls=%async_computation.6 | async-start | bytes 6553600 | tf_op jit(solution)/shard_map/all_gather | solution.py:117
  324.8 118.6 %reduce-scatter.2.cloned.1.call-start = ((), (), s32[]{:S(2)}) async-start(), calls=%async_computation.7 | async-start | bytes 6553600 | tf_op jit(solution)/shard_map/reduce_scatter | solution.py:122
  391.9 88.2 %copy-start.4 = (f32[128,2]{0,1:T(2,128)S(1)}, f32[128,2]{0,1:T(2,128)}, u32[]{:S(2)}) copy-start(f32[128,2]{0,1:T(2,128)} %param.24) | copy-start | bytes 3076
Sparse Core Ops, SparseCore 0:
  9.4 42.1 all-gather.5
  53.6 38.1 all-gather.3
  325.0 38.7 all-gather.7
  392.0 51.3 reduce-scatter.1
where the time goes:
time: 489 us; the launch traced here: 488 us
  blocking collectives  255 us (52%)
  waiting for transfers between devices  144 us (29%)
  matrix products  34.4 us (7%)
  other arithmetic  19.2 us (4%)
  local copies, waits for them, and re-layouts  18.3 us (4%)
  between operations  13.2 us (3%)
    all_to_all x1, blocking collectives, shards(): lax.all_to_all(outgoing, 'sp', split_axis=0, concat_axis=0, tiled=True)  190 us
    reduce_scatter x1, waiting for transfers between devices, shards(): lax.psum_scatter(lax.optimization_barrier(partial_value.astype(jnp.bfloat...  51.5 us
    all_gather x1, waiting for transfers between devices, shards(): value_piece = lax.all_gather(values, 'sp', axis=0, tiled=True)  40.3 us
    all_gather x1, waiting for transfers between devices, shards(): row_block = lax.all_gather(arrived, 'tp', axis=0, tiled=True)  38.8 us
    all_to_all x1, blocking collectives, shards(): lax.all_to_all(summed, 'sp', split_axis=0, concat_axis=0, tiled=True)  36.7 us
    all_gather x1, blocking collectives, shards(): bias_piece = lax.all_gather(key_bias, 'sp', axis=0, tiled=True)  28.3 us
    dot_general x1, matrix products, shards(): jnp.dot(hidden, down_weight[0], preferred_element_type=jnp.float32)  18 us
    another operation x4, other arithmetic  10.3 us
  transfers between devices with their start and end apart: 5, of which 5 were waited for; matrix products, arithmetic and copies ran while one was open for 1% of the time, Pallas kernels for 0%

commit v1 on v0

--- a/solution.py
+++ b/solution.py
@@ -2,11 +2,25 @@
 import jax.numpy as jnp
 from jax import lax
 from jax.sharding import PartitionSpec as P
+from jax.lax import axis_index, axis_size, ppermute
 
 HEAD_DIM = 64
 TOP = 2
 SPAN = 512
 epsilon = 1e-06
+
+
+def search_the_classes(sheet):
+    n_all = axis_size("sp")
+    finding = sheet
+    column = [finding]
+    block_last = sorted(((pp, (pp + 1) % n_all) for pp in range(n_all)))
+    for num in range(1, n_all):
+        finding = ppermute(finding, axis_name="sp", perm=block_last)
+        column.insert(0, finding)
+    inter = jnp.concatenate(column, 0)
+    b_now = axis_index("sp")
+    return jnp.roll(inter, (b_now + 1) * sheet.shape[0], 0)
 
 
 def shards(
@@ -66,7 +80,7 @@
         jnp.zeros((slot_count, shard_len, local_heads), jnp.float32),
     )
     key_piece = lax.all_gather(keys, "sp", axis=0, tiled=True)
-    value_piece = lax.all_gather(values, "sp", axis=0, tiled=True)
+    value_piece = search_the_classes(values)
     bias_piece = lax.all_gather(key_bias, "sp", axis=0, tiled=True)
     span_total = key_piece.shape[0] // SPAN
 

time: 489 us -> 517 us (1.057)
  blocking collectives: 255 us -> 277 us
  waiting for transfers between devices: 144 us -> 133 us
  local copies, waits for them, and re-layouts: 18.3 us -> 24.5 us
    all_gather x1 -> x0, waiting for transfers between devices: 40.3 us -> none  [shards(): value_piece = lax.all_gather(values, 'sp', axis=0, tiled=True)]
    ppermute x0 -> x7, waiting for transfers between devices: none -> 38.4 us  [search_the_classes(): finding = ppermute(finding, axis_name='sp', perm=block_last)]
    all_to_all x1, blocking collectives: 190 us -> 213 us  [shards(): lax.all_to_all(outgoing, 'sp', split_axis=0, concat_axis=0, tiled=True)]
    all_gather x1, waiting for transfers between devices: 9.23 us -> 0.02 us  [shards(): key_piece = lax.all_gather(keys, 'sp', axis=0, tiled=True)]
  transfers between devices with their start and end apart: 5 -> 11, of which waited for: 5 -> 9; matrix products, arithmetic and copies ran while one was open for 1% -> 1% of each run, Pallas kernels for 0% -> 0%
where the time goes in v1:
time: 517 us; the launch traced here: 515 us
  blocking collectives  277 us (54%)
  waiting for transfers between devices  133 us (26%)
  matrix products  36 us (7%)
  local copies, waits for them, and re-layouts  24.5 us (5%)
  other arithmetic  21.9 us (4%)
  between operations  13.4 us (3%)
  starting transfers between devices  8.68 us (2%)
    all_to_all x1, blocking collectives, shards(): lax.all_to_all(outgoing, 'sp', split_axis=0, concat_axis=0, tiled=True)  213 us
    reduce_scatter x1, waiting for transfers between devices, shards(): lax.psum_scatter(lax.optimization_barrier(partial_value.astype(jnp.bfloat...  51.5 us
    all_gather x1, waiting for transfers between devices, shards(): row_block = lax.all_gather(arrived, 'tp', axis=0, tiled=True)  38.8 us
    ppermute x7, waiting for transfers between devices, search_the_classes(): finding = ppermute(finding, axis_name='sp', perm=block_last)  38.4 us
    all_to_all x1, blocking collectives, shards(): lax.all_to_all(summed, 'sp', split_axis=0, concat_axis=0, tiled=True)  36.7 us
    all_gather x1, blocking collectives, shards(): bias_piece = lax.all_gather(key_bias, 'sp', axis=0, tiled=True)  27.4 us
    dot_general x1, matrix products, shards(): jnp.dot(hidden, down_weight[0], preferred_element_type=jnp.float32)  18 us
    another operation x4, other arithmetic  10.9 us
  transfers between devices with their start and end apart: 11, of which 9 were waited for; matrix products, arithmetic and copies ran while one was open for 1% of the time, Pallas kernels for 0%

profile of v1, /device:TPU:0, one launch (start us, length us, event | category | flops | bytes accessed | tf_op | source)
XLA Modules:
  0.0 514.7 jit_solution(582905120616945762)
XLA Ops:
  6.5 1.2 copy.70
  7.7 3.0 collective-permute-start
  10.7 6.5 %collective-permute-done = bf16[512,128]{0,1:T(8,128)(2,1)S(1)} collective-permute-done((bf16[512,128]{0,1:T(8,128)(2,1)S(1)}, bf16[512,128]{0,1:T(8,128)(2,1)S(1)}, u32[]{:S(2)}, u32[]{:S(2)}) %collective-permute-start) | collective-permute-done | bytes 131104 | tf_op jit(solution)/shard_map/ppermute | solution.py:19
  17.3 7.7 %collective-permute-done.1 = bf16[512,128]{0,1:T(8,128)(2,1)S(1)} collective-permute-done((bf16[512,128]{0,1:T(8,128)(2,1)S(1)}, bf16[512,128]{0,1:T(8,128)(2,1)S(1)}, u32[]{:S(2)}, u32[]{:S(2)}) %collective-permute-start.1) | collective-permute-done | bytes 131104 | tf_op jit(solution)/shard_map/ppermute | solution.py:19
  24.9 7.7 %collective-permute-done.2 = bf16[512,128]{0,1:T(8,128)(2,1)S(1)} collective-permute-done((bf16[512,128]{0,1:T(8,128)(2,1)S(1)}, bf16[512,128]{0,1:T(8,128)(2,1)S(1)}, u32[]{:S(2)}, u32[]{:S(2)}) %collective-permute-start.2) | collective-permute-done | bytes 131104 | tf_op jit(solution)/shard_map/ppermute | solution.py:19
  32.6 1.7 copy.73
  35.2 5.0 collective-permute-done.3
  40.8 7.2 %collective-permute-done.4 = bf16[512,128]{0,1:T(8,128)(2,1)S(1)} collective-permute-done((bf16[512,128]{0,1:T(8,128)(2,1)S(1)}, bf16[512,128]{0,1:T(8,128)(2,1)S(1)}, u32[]{:S(2)}, u32[]{:S(2)}) %collective-permute-start.4) | collective-permute-done | bytes 131104 | tf_op jit(solution)/shard_map/ppermute | solution.py:19
  48.8 1.7 copy.74
  50.5 27.4 %all_gather.10 = bf16[4096,2]{0,1:T(2,128)(2,1)} all-gather(bf16[512,2]{0,1:T(2,128)(2,1)} %param.19), channel_id=1, replica_groups=mesh['sp'=8,'tp'=4] {'sp'}, dimensions={0}, use_global_device_ids=true | all-gather | bytes 18432 | tf_op jit(solution)/shard_map/all_gather | solution.py:84
  77.8 2.1 collective-permute-start.6
  80.0 1.3 multiply_add_fusion.1
  81.2 4.3 collective-permute-done.6
  86.6 1.6 broadcast_in_dim.56
  88.1 36.7 %while.18 = (s32[]{:T(128)}, f32[8,512,2,64]{1,3,2,0:T(8,128)}, f32[8,512,2]{1,2,0:T(2,128)}, s32[]{:T(128)}, bf16[4096,128]{0,1:T(8,128)(2,1)S(1)}, /*index=5*/...) while((s32[]{:T(128)}, f32[8,512,2,64]{1,3,2,0:T(8,128)}, ...), condition=%wide.region_6.7_spmd.clone, body=%wide.region_0.6_spmd.clone.sunk | while | flops 218906624 | bytes 42543728 | solution.py:106
  88.1 25.8 %conditional.3 = (f32[1,512,2,64]{1,3,2,0:T(8,128)S(1)}, f32[1,512,2]{1,2,0:T(2,128)S(1)}) conditional(s32[]{:T(128)} %convert_element_type.94, () %tuple.60, (s32[]{:T(128)}, bf16[4096,128]{0,1:T(8,128)(2,1)S(1)}, s32[]{:T(128)}, bf16[4096,128]{0,1:T(8,128)(2,1)}, bf16[512,2,64]{0,2,1:T(8,128)(2,1)}, /*index=5*/bf16[4096,2]{0,1:T(2,128)(2,1)}, ...), branch_computations={%region_1.1_spmd, %region_2.5_spmd} | conditional | flops 218906624 | bytes 42008788 | solution.py:99
  90.0 4.6 fusion.15
  94.6 9.6 %fusion.13 = f32[512,2,4,128]{0,2,1,3:T(4,128)S(1)} fusion(f32[512,2,4,128]{0,3,2,1:T(8,128)S(1)} %bitcast.89), kind=kOutput, calls=%fused_computation.18 | output fusion | flops 66584576 | bytes 4194304 | tf_op jit(solution)/shard_map/reduce-window
  104.2 1.3 copy-done.1
  106.9 1.8 broadcast_add_fusion
  108.8 1.2 copy.68
  110.4 3.2 fusion.6
  125.7 1.9 multiply_reduce_fusion
  128.2 3.5 all-to-all-start
  131.8 4.5 all-to-all-done
  136.3 1.6 multiply_reduce_fusion.1
  138.5 212.7 %all_to_all.40 = bf16[8,40,2048]{2,1,0:T(8,128)(2,1)} all-to-all(bf16[8,40,2048]{2,1,0:T(8,128)(2,1)S(1)} %bitcast.92), channel_id=1, replica_groups=mesh['sp'=8,'tp'=4] {'sp'}, dimensions={0} | all-to-all | bytes 2621440 | tf_op jit(solution)/shard_map/all_to_all | solution.py:130
  351.2 38.8 %all-gather.5.cloned.1.call-done = bf16[1280,2048]{1,0:T(8,128)(2,1)} async-done(((bf16[320,2048]{1,0:T(8,128)(2,1)}), bf16[1280,2048]{1,0:T(8,128)(2,1)}) %all-gather.5.cloned.1.call-update) | async-done | bytes 5242896 | tf_op jit(solution)/shard_map/all_gather | solution.py:131
  390.1 10.2 %fusion.18 = f32[1280,1024]{1,0:T(8,128)} fusion(bf16[1280,2048]{1,0:T(8,128)(2,1)} %all-gather.5.cloned.1.call-done, bf16[1,2048,1024]{2,1,0:T(8,128)(2,1)} %param.25), kind=kOutput, calls=%fused_computation.37 | convolution fusion | flops 5368709120 | bytes 14680064 | tf_op jit(solution)/shard_map/dot_general | solution.py:132
  400.3 18.0 %convolution_convert_fusion = bf16[1280,2048]{1,0:T(8,128)(2,1)} fusion(bf16[1,1024,2048]{2,1,0:T(8,128)(2,1)} %param.27, f32[1280,1024]{1,0:T(8,128)} %fusion.18, bf16[1280,2048]{1,0:T(8,128)(2,1)} %all-gather.5.cloned.1.call-done, bf16[1,2048,1024]{2,1,0:T(8,128)(2,1)} %param.26), kind=kOutput, calls=%fused_computation.33 | convolution fusion | flops 10747904000 | bytes 24117248 | tf_op jit(solution)/shard_map/dot_general | solution.py:135
  418.2 51.5 %reduce-scatter.2.cloned.1.call-done = bf16[320,2048]{1,0:T(8,128)(2,1)} async-done(((bf16[1280,2048]{1,0:T(8,128)(2,1)}), bf16[320,2048]{1,0:T(8,128)(2,1)}) %reduce-scatter.2.cloned.1.call-update) | async-done | bytes 1310736 | tf_op jit(solution)/shard_map/reduce_scatter | solution.py:136
  469.7 36.7 %all_to_all.41 = bf16[8,40,2048]{2,1,0:T(8,128)(2,1)S(1)} all-to-all(bf16[8,40,2048]{2,1,0:T(8,128)(2,1)} %bitcast.95), channel_id=1, replica_groups=mesh['sp'=8,'tp'=4] {'sp'}, dimensions={0} | all-to-all | bytes 2621440 | tf_op jit(solution)/shard_map/all_to_all | solution.py:144
  (120 shorter events, 22.0 us)
Async XLA Ops:
  6.5 129.7 %copy-start = (bf16[512,2048]{1,0:T(8,128)(2,1)S(1)}, bf16[512,2048]{1,0:T(8,128)(2,1)}, u32[]{:S(2)}) copy-start(bf16[512,2048]{1,0:T(8,128)(2,1)} %param.21) | copy-start | bytes 6291460
  6.5 79.4 %all-gather.3.cloned.1.call-start = ((), (), s32[]{:S(2)}) async-start(), calls=%async_computation.4 | async-start | bytes 1179648 | tf_op jit(solution)/shard_map/all_gather | solution.py:82
  7.7 9.6 %collective-permute-start = (bf16[512,128]{0,1:T(8,128)(2,1)S(1)}, bf16[512,128]{0,1:T(8,128)(2,1)S(1)}, u32[]{:S(2)}, u32[]{:S(2)}) collective-permute-start(bf16[512,128]{0,1:T(8,128)(2,1)S(1)} %copy.70), channel_id=1, source_target_pairs={{0,4},{4,8},{8,12},{12,16},{16,20},{20,24},{24,28},{28,0},{1,5},{5... | collective-permute-start | bytes 393224 | tf_op jit(solution)/shard_map/ppermute | solution.py:19
  17.3 7.7 %collective-permute-start.1 = (bf16[512,128]{0,1:T(8,128)(2,1)S(1)}, bf16[512,128]{0,1:T(8,128)(2,1)S(1)}, u32[]{:S(2)}, u32[]{:S(2)}) collective-permute-start(bf16[512,128]{0,1:T(8,128)(2,1)S(1)} %collective-permute-done), channel_id=1, source_target_pairs={{0,4},{4,8},{8,12},{12,16},{16,20},{20,24},{24,28},{28,0},{1,5},{5... | collective-permute-start | bytes 393224 | tf_op jit(solution)/shard_map/ppermute | solution.py:19
  24.9 7.7 %collective-permute-start.2 = (bf16[512,128]{0,1:T(8,128)(2,1)S(1)}, bf16[512,128]{0,1:T(8,128)(2,1)S(1)}, u32[]{:S(2)}, u32[]{:S(2)}) collective-permute-start(bf16[512,128]{0,1:T(8,128)(2,1)S(1)} %collective-permute-done.1), channel_id=1, source_target_pairs={{0,4},{4,8},{8,12},{12,16},{16,20},{20,24},{24,28},{28,0},{1,5},{5... | collective-permute-start | bytes 393224 | tf_op jit(solution)/shard_map/ppermute | solution.py:19
  32.6 7.7 %collective-permute-start.3 = (bf16[512,128]{0,1:T(8,128)(2,1)S(1)}, bf16[512,128]{0,1:T(8,128)(2,1)S(1)}, u32[]{:S(2)}, u32[]{:S(2)}) collective-permute-start(bf16[512,128]{0,1:T(8,128)(2,1)S(1)} %collective-permute-done.2), channel_id=1, source_target_pairs={{0,4},{4,8},{8,12},{12,16},{16,20},{20,24},{24,28},{28,0},{1,5},{5... | collective-permute-start | bytes 393224 | tf_op jit(solution)/shard_map/ppermute | solution.py:19
  40.3 7.8 %collective-permute-start.4 = (bf16[512,128]{0,1:T(8,128)(2,1)S(1)}, bf16[512,128]{0,1:T(8,128)(2,1)S(1)}, u32[]{:S(2)}, u32[]{:S(2)}) collective-permute-start(bf16[512,128]{0,1:T(8,128)(2,1)S(1)} %collective-permute-done.3), channel_id=1, source_target_pairs={{0,4},{4,8},{8,12},{12,16},{16,20},{20,24},{24,28},{28,0},{1,5},{5... | collective-permute-start | bytes 393224 | tf_op jit(solution)/shard_map/ppermute | solution.py:19
  48.1 29.8 %collective-permute-start.5 = (bf16[512,128]{0,1:T(8,128)(2,1)S(1)}, bf16[512,128]{0,1:T(8,128)(2,1)S(1)}, u32[]{:S(2)}, u32[]{:S(2)}) collective-permute-start(bf16[512,128]{0,1:T(8,128)(2,1)S(1)} %collective-permute-done.4), channel_id=1, source_target_pairs={{0,4},{4,8},{8,12},{12,16},{16,20},{20,24},{24,28},{28,0},{1,5},{5... | collective-permute-start | bytes 393224 | tf_op jit(solution)/shard_map/ppermute | solution.py:19
  77.8 7.7 %collective-permute-start.6 = (bf16[512,128]{0,1:T(8,128)(2,1)S(1)}, bf16[512,128]{0,1:T(8,128)(2,1)S(1)}, u32[]{:S(2)}, u32[]{:S(2)}) collective-permute-start(bf16[512,128]{0,1:T(8,128)(2,1)S(1)} %collective-permute-done.5), channel_id=1, source_target_pairs={{0,4},{4,8},{8,12},{12,16},{16,20},{20,24},{24,28},{28,0},{1,5},{5... | collective-permute-start | bytes 393224 | tf_op jit(solution)/shard_map/ppermute | solution.py:19
  89.7 4.8 copy-start.3
  104.2 1.3 copy-start.1
  108.8 1.6 copy-start.2
  108.8 1.6 copy-start.4
  110.4 3.5 copy-start.5
  124.8 7.0 %copy-start.7 = (s32[128,2]{0,1:T(2,128)S(1)}, s32[128,2]{0,1:T(2,128)}, u32[]{:S(2)}) copy-start(s32[128,2]{0,1:T(2,128)} %multiply_add_fusion.1) | copy-start | bytes 3076
  128.2 9.6 %copy-start.6 = (f32[2048]{0:T(1024)S(1)}, f32[2048]{0:T(1024)}, u32[]{:S(2)}) copy-start(f32[2048]{0:T(1024)} %param.22) | copy-start | bytes 24580
  128.2 8.0 %all-to-all-start = ((bf16[4,128,128]{1,2,0:T(8,128)(2,1)}), bf16[4,128,128]{1,2,0:T(8,128)(2,1)S(1)}, u32[]{:S(2)}, u32[]{:S(2)}) async-start(bf16[4,128,128]{1,2,0:T(8,128)(2,1)} %copy.75), calls=%async_computation | async-start | bytes 262144 | tf_op jit(solution)/shard_map/all_to_all | solution.py:110
  131.7 258.3 %all-gather.5.cloned.1.call-start = ((), (), s32[]{:S(2)}) async-start(), calls=%async_computation.5 | async-start | bytes 6553600 | tf_op jit(solution)/shard_map/all_gather | solution.py:131
  351.2 118.6 %reduce-scatter.2.cloned.1.call-start = ((), (), s32[]{:S(2)}) async-start(), calls=%async_computation.6 | async-start | bytes 6553600 | tf_op jit(solution)/shard_map/reduce_scatter | solution.py:136
  418.2 88.2 %copy-start.8 = (f32[128,2]{0,1:T(2,128)S(1)}, f32[128,2]{0,1:T(2,128)}, u32[]{:S(2)}) copy-start(f32[128,2]{0,1:T(2,128)} %param.24) | copy-start | bytes 3076
Sparse Core Ops, SparseCore 0:
  34.4 42.6 all-gather.2
  351.3 38.7 all-gather.4
  418.4 51.3 reduce-scatter.1
